TPU v7x, 32 devices: a whole 2x2x4 slice. The times are simulated.
32 devices in a mesh: sp: 4 (over y, x), tp: 8 (over z, core).
Axes of the slice: x: 2, y: 2, z: 4, core: 2. Of those that a mesh axis runs over, the one named last changes fastest.
Arguments:
- queries: bfloat16 [1536, 2048], P('sp', 'tp'), may hold values from -6 to 6
- keys: bfloat16 [1536, 2048], P('sp', 'tp'), may hold values from -6 to 6
- values: bfloat16 [1536, 2048], P('sp', 'tp'), may hold values from -6 to 6
- key_bias: bfloat16 [1536, 32], P('sp', 'tp'), may hold values from -16 to 0
- head_gain: float32 [32, 64], P('tp'), may hold values from 0.1 to 1.9
- out_weight: bfloat16 [2048, 2048], P('tp'), may hold values from -0.125 to 0.125
- residual: bfloat16 [1536, 2048], P(('sp', 'tp')), may hold values from -6 to 6
- norm_gain: float32 [2048], replicated, may hold values from 0.1 to 1.9
- gate_proj: bfloat16 [4, 2048, 7168], P('sp', None, 'tp'), may hold values from -0.125 to 0.125
- up_proj: bfloat16 [4, 2048, 7168], P('sp', None, 'tp'), may hold values from -0.125 to 0.125
- down_proj: bfloat16 [4, 7168, 2048], P('sp', 'tp'), may hold values from -0.0625 to 0.0625
- expert_choice: int32 [1536, 2], P(('sp', 'tp')), may hold values from 0 to 3, all different within a row; in each aligned block of 48 rows (0 to 47, 48 to 95, ...) at most 48 rows name the same one
- expert_weights: float32 [1536, 2], P(('sp', 'tp')), may hold values from 0.2 to 1
Outputs:
- layer_out: bfloat16 [1536, 2048], P(('sp', 'tp'))
Inputs may be any that keep to these rules, and one draw needn't show every extreme that they name: `expert_choice`: in each aligned block of 48 rows (the rows of one device), no expert is named more than 48 times; the two experts of a row differ.
All inputs are finite; a program needn't handle non-finite values.
Results may differ from a plain program's by a relative error of at most 0.019.
Values may be sent and summed in bfloat16 or wider, within the bound.
A program may use at most 128 MiB of HBM per device.

v0:
```python
import jax
import jax.numpy as jnp
from jax import lax
from jax.sharding import PartitionSpec as P

epsilon = 1e-06


def rms_scaled(values_in):
    return values_in * lax.rsqrt(jnp.mean(values_in * values_in, axis=-1, keepdims=True) + epsilon)


def expert_partial(row_block, gate_matrix, up_matrix, down_matrix):
    gate_part = jnp.dot(row_block, gate_matrix, preferred_element_type=jnp.float32)
    up_part = jnp.dot(row_block, up_matrix, preferred_element_type=jnp.float32)
    hidden = (jax.nn.silu(gate_part) * up_part).astype(jnp.bfloat16)
    return jnp.dot(hidden, down_matrix, preferred_element_type=jnp.float32)


def choice_ranks(routes, experts_all):
    flat_routes = routes.reshape(routes.shape[:-2] + (-1,))
    onehot = (flat_routes[..., None] == jnp.arange(experts_all, dtype=jnp.int32)).astype(jnp.int32)
    before = jnp.cumsum(onehot, axis=-2) - onehot
    return jnp.sum(before * onehot, axis=-1).reshape(routes.shape)


def slot_tokens(slot_index, targets, missing):
    flat_slots = slot_index.reshape(-1)
    owners = jnp.arange(flat_slots.shape[0], dtype=jnp.int32) // 2
    matches = flat_slots[None, :] == jnp.arange(targets, dtype=jnp.int32)[:, None]
    owner_found = jnp.sum(jnp.where(matches, owners[None, :], 0), axis=1)
    return jnp.where(jnp.any(matches, axis=1), owner_found, missing)


def on_device(
    queries,
    keys,
    values,
    key_bias,
    head_gain,
    out_weight,
    residual,
    norm_gain,
    gate_proj,
    up_proj,
    down_proj,
    expert_choice,
    expert_weights,
):
    rows_own = queries.shape[0]
    heads_here = head_gain.shape[0]
    head_size = head_gain.shape[1]
    model_width = out_weight.shape[1]
    seq_devices = lax.axis_size("sp")
    head_devices = lax.axis_size("tp")
    own_start = lax.axis_index("sp") * rows_own
    query_pos = own_start + jnp.arange(rows_own, dtype=jnp.int32)
    query_heads = queries.reshape(rows_own, heads_here, head_size)

    def key_block(slot_state, key_rows, value_rows, bias_rows, key_start):
        key_heads = key_rows.reshape(rows_own, heads_here, head_size)
        value_heads = value_rows.reshape(rows_own, heads_here, head_size)
        scores = jnp.einsum(
            "qhd,khd->hqk", query_heads, key_heads, preferred_element_type=jnp.float32
        ) * head_size ** (-0.5)
        scores = scores + bias_rows.astype(jnp.float32).T[:, None, :]
        key_pos = key_start + jnp.arange(rows_own, dtype=jnp.int32)
        earlier = (key_pos[None, :] < query_pos[:, None])[None, :, :]
        log_drops = jnp.where(earlier, jax.nn.log_sigmoid(-scores), 0.0)
        suffix = lax.cumsum(log_drops, axis=2, reverse=True) - log_drops
        within = jnp.where(earlier, jnp.exp(jax.nn.log_sigmoid(scores) + suffix), 0.0).astype(
            jnp.bfloat16
        )
        block_part = jnp.einsum(
            "hqk,khd->qhd", within, value_heads, preferred_element_type=jnp.float32
        )
        block_index = key_start // rows_own
        sums_new = lax.dynamic_update_index_in_dim(
            slot_state[0], block_part.reshape(rows_own, heads_here * head_size), block_index, 0
        )
        totals_new = lax.dynamic_update_index_in_dim(
            slot_state[1], jnp.sum(log_drops, axis=2), block_index, 0
        )
        return (sums_new, totals_new)

    empty_state = (
        jnp.zeros((seq_devices, rows_own, heads_here * head_size), jnp.float32),
        jnp.zeros((seq_devices, heads_here, rows_own), jnp.float32),
    )
    key_piece = lax.all_gather(keys, "sp", axis=0, tiled=True)
    value_piece = lax.all_gather(values, "sp", axis=0, tiled=True)
    bias_piece = lax.all_gather(key_bias, "sp", axis=0, tiled=True)

    def visit(block_count, state_in):
        offset = block_count * rows_own

        def take_rows(array):
            return lax.dynamic_slice_in_dim(array, offset, rows_own, 0)

        def compute(state_now):
            return key_block(
                state_now,
                take_rows(key_piece),
                take_rows(value_piece),
                take_rows(bias_piece),
                offset,
            )

        def keep(state_now):
            return state_now

        return lax.cond(offset <= own_start, compute, keep, state_in)

    block_sums, totals = lax.fori_loop(0, key_piece.shape[0] // rows_own, visit, empty_state)
    carried = jnp.sum(totals, axis=0, keepdims=True) - jnp.cumsum(totals, axis=0)
    factors = jnp.exp(carried).transpose(0, 2, 1)[..., None]
    mixture = jnp.sum(
        factors * block_sums.reshape(seq_devices, rows_own, heads_here, head_size), axis=0
    )
    attended = (
        (rms_scaled(mixture) * head_gain)
        .astype(jnp.bfloat16)
        .reshape(rows_own, heads_here * head_size)
    )
    row_share = rows_own // head_devices
    merged = lax.all_to_all(attended, "tp", split_axis=0, concat_axis=1, tiled=True)
    projected = jnp.dot(
        merged,
        lax.all_gather(out_weight, "tp", axis=0, tiled=True),
        preferred_element_type=jnp.float32,
    )
    stream = (residual.astype(jnp.float32) + projected).astype(jnp.bfloat16)
    normed = (rms_scaled(stream.astype(jnp.float32)) * norm_gain).astype(jnp.bfloat16)
    local_experts = gate_proj.shape[0]
    experts_all = local_experts * seq_devices
    capacity = 4 * rows_own // (head_devices * experts_all)
    own_slots = expert_choice * capacity + choice_ranks(expert_choice, experts_all)
    wanted = slot_tokens(own_slots, experts_all * capacity, row_share)
    outgoing = jnp.take(normed, wanted, axis=0, mode="fill", fill_value=0)
    arrived = lax.all_to_all(
        outgoing.reshape(seq_devices, local_experts, capacity, model_width),
        "sp",
        split_axis=0,
        concat_axis=0,
        tiled=True,
    )
    row_piece = lax.all_gather(arrived, "tp", axis=0, tiled=True)
    count_rows = row_piece.shape[0]
    partials = jnp.stack(
        [
            expert_partial(
                row_piece[:, 0].reshape(-1, model_width), gate_proj[0], up_proj[0], down_proj[0]
            ).reshape(count_rows, capacity, model_width)
        ],
        axis=1,
    )
    summed = lax.psum_scatter(partials.astype(jnp.bfloat16), "tp", scatter_dimension=0, tiled=True)
    returned = lax.all_to_all(summed, "sp", split_axis=0, concat_axis=0, tiled=True).reshape(
        experts_all * capacity, model_width
    )
    picked = jnp.take(returned, own_slots, axis=0).astype(jnp.float32)
    combined = jnp.sum(expert_weights[:, :, None] * picked, axis=1)
    return (stream.astype(jnp.float32) + combined).astype(jnp.bfloat16)


def solution(mesh):
    placed = (
        P("sp", "tp"),
        P("sp", "tp"),
        P("sp", "tp"),
        P("sp", "tp"),
        P("tp", None),
        P("tp", None),
        P(("sp", "tp"), None),
        P(),
        P("sp", None, "tp"),
        P("sp", None, "tp"),
        P("sp", "tp", None),
        P(("sp", "tp"), None),
        P(("sp", "tp"), None),
    )
    return jax.shard_map(
        on_device, mesh=mesh, in_specs=placed, out_specs=P(("sp", "tp"), None), check_vma=False
    )
```

profile of v0, /device:TPU:0, one launch (start us, length us, event | category | flops | bytes accessed | tf_op | source)
XLA Modules:
  0.0 380.5 jit_solution(13210839301603181166)
XLA Ops:
  6.5 0.7 all-gather.3.cloned.1.call-update
  7.3 1.1 copy.81
  8.4 1.1 copy.82
  9.4 1.7 copy.83
  11.2 11.0 %all_gather.17 = bf16[1536,4]{0,1:T(4,128)(2,1)} all-gather(bf16[384,4]{0,1:T(4,128)(2,1)} %param.20), channel_id=1, replica_groups=mesh['sp'=4,'tp'=8] {'sp'}, dimensions={0}, use_global_device_ids=true | all-gather | bytes 15360 | tf_op jit(solution)/shard_map/all_gather | solution.py:92
  22.2 12.4 %all_gather.15 = bf16[1536,256]{0,1:T(8,128)(2,1)} all-gather(bf16[384,256]{0,1:T(8,128)(2,1)S(1)} %copy.81), channel_id=1, replica_groups=mesh['sp'=4,'tp'=8] {'sp'}, dimensions={0}, use_global_device_ids=true | all-gather | bytes 983040 | tf_op jit(solution)/shard_map/all_gather | solution.py:91
  34.5 13.4 %all_gather.16 = bf16[1536,256]{0,1:T(8,128)(2,1)} all-gather(bf16[384,256]{0,1:T(8,128)(2,1)S(1)} %copy.82), channel_id=1, replica_groups=mesh['sp'=4,'tp'=8] {'sp'}, dimensions={0}, use_global_device_ids=true | all-gather | bytes 983040 | tf_op jit(solution)/shard_map/all_gather | solution.py:90
  47.9 1.3 broadcast_in_dim.84
  49.2 0.6 broadcast_in_dim.85
  49.8 28.2 %while.17 = (s32[]{:T(128)}, f32[4,384,256]{1,2,0:T(8,128)}, f32[4,4,384]{2,1,0:T(4,128)}, s32[]{:T(128)}, bf16[1536,256]{0,1:T(8,128)(2,1)}, /*index=5*/bf16[15...) while((s32[]{:T(128)}, f32[4,384,256]{1,2,0:T(8,128)}, ...), condition=%wide.region_6.7_spmd.clone.clone, body=%wide.region_0.6_spmd.clone.clone.sunk | while | flops 246117120 | bytes 38572464 | solution.py:114
  49.8 28.0 %conditional.4 = ((f32[4,384,256]{1,2,0:T(8,128)}, f32[4,4,384]{2,1,0:T(4,128)})) conditional(s32[]{:T(128)} %convert_element_type.76, (f32[4,384,256]{1,2,0:T(8,128)}, f32[4,4,384]{2,1,0:T(4,128)}) %tuple.53, (s32[]{:T(128)}, bf16[1536,256]{0,1:T(8,128)(2,1)}, s32[]{:T(128)}, bf16[1536,256]{0,1:T(8,128)(2,1)}, bf16[384,4,64]{0,2,1:T(8,128)(2,1)}, ...), branch_computations={%region_1.0_spmd, %region_2.5_spmd} | conditional | flops 246117120 | bytes 38570716 | solution.py:112
  49.8 1.1 constant_dynamic-slice_fusion
  50.8 0.7 convert_bitcast_fusion
  51.5 0.1 broadcast_compare_fusion
  51.7 4.3 %fusion.15 = (f32[4,384]{1,0:T(4,128)S(1)}, f32[4,384,384]{1,2,0:T(8,128)S(1)}, f32[4,384,384]{2,1,0:T(8,128)}) fusion(f32[4,384]{1,0:T(4,128)S(1)} %convert_bitcast_fusion, pred[384,384]{0,1:T(8,128)(4,1)S(1)} %broadcast_compare_fusion, bf16[384,4,64]{0,2,1:T(8,128)(2,1)S(1)} %bitcast.92, bf16[384,4,64]{0,2,1:T(8,128)(2,1)} %get-tuple-element.177), kind=kOutput, calls=%fused_computation.33 | convolution fusion | flops 81984000 | bytes 5271552 | tf_op jit(solution)/shard_map/while/body/eval_jaxpr/cond/branch_1_fun/qhd,khd->hqk/dot_general | solution.py:63
  56.0 14.0 %fusion.2 = f32[4,384,3,128]{1,2,3,0:T(4,128)S(1)} fusion(f32[4,384,3,128]{1,3,2,0:T(8,128)S(1)} %bitcast.88), kind=kOutput, calls=%fused_computation.5 | output fusion | flops 74907648 | bytes 4718592 | tf_op jit(solution)/shard_map/reduce-window
  70.1 0.5 broadcast_add_fusion
  70.6 0.2 copy.79
  70.9 1.5 copy-done
  72.3 3.6 fusion.8
  76.0 0.3 fusion.27
  76.3 0.8 constant_dynamic-update-slice_fusion
  77.1 0.6 bitcast_dynamic-update-slice_fusion
  78.0 0.8 reduce_sum.74
  78.7 0.8 fusion.24
  79.5 1.6 fusion.22
  81.1 0.2 copy.84
  81.3 0.1 copy.85
  81.5 0.5 mul.104
  81.9 0.5 mul.105
  82.5 0.7 multiply_convert_fusion.2
  83.2 4.8 %all-to-all-start = ((bf16[8,48,256]{2,1,0:T(8,128)(2,1)}), bf16[8,48,256]{2,1,0:T(8,128)(2,1)S(1)}, u32[]{:S(2)}, u32[]{:S(2)}) async-start(bf16[8,48,256]{2,1,0:T(8,128)(2,1)} %multiply_convert_fusion.2), calls=%async_computation | async-start | bytes 393216 | tf_op jit(solution)/shard_map/all_to_all | solution.py:126
  88.5 0.2 select_reduce_fusion.1
  89.5 6.8 %all-to-all-done = bf16[8,48,256]{2,1,0:T(8,128)(2,1)S(1)} async-done(((bf16[8,48,256]{2,1,0:T(8,128)(2,1)}), bf16[8,48,256]{2,1,0:T(8,128)(2,1)S(1)}, u32[]{:S(2)}, u32[]{:S(2)}) %all-to-all-start) | async-done | bytes 196640 | tf_op jit(solution)/shard_map/all_to_all | solution.py:126
  96.4 5.1 %multiply_reduce_fusion.1 = (f32[48]{0:T(128)S(1)}, f32[48,2048]{1,0:T(8,128)S(1)}) fusion(bf16[48,2048]{1,0:T(8,128)(2,1)S(1)} %bitcast.94, bf16[2048,2048]{1,0:T(8,128)(2,1)} %all-gather.3.cloned.1.call-done, bf16[48,2048]{1,0:T(8,128)(2,1)S(1)} %copy-done.1), kind=kOutput, calls=%fused_computation.54 | convolution fusion | flops 403242944 | bytes 9175232 | tf_op jit(solution)/shard_map/dot_general | solution.py:127
  101.6 1.1 gather_fusion
  102.9 96.4 %all_to_all.26 = bf16[4,1,48,2048]{3,2,1,0:T(8,128)(2,1)} all-to-all(bf16[4,1,48,2048]{3,2,1,0:T(8,128)(2,1)S(1)} %broadcast_select_fusion), channel_id=1, replica_groups=mesh['sp'=4,'tp'=8] {'sp'}, dimensions={0} | all-to-all | bytes 1572864 | tf_op jit(solution)/shard_map/all_to_all | solution.py:140
  199.4 63.5 %all-gather.5.cloned.1.call-done = bf16[32,1,48,2048]{3,2,1,0:T(8,128)(2,1)} async-done(((bf16[4,1,48,2048]{3,2,1,0:T(8,128)(2,1)}), bf16[32,1,48,2048]{3,2,1,0:T(8,128)(2,1)}) %all-gather.5.cloned.1.call-update) | async-done | bytes 6291472 | tf_op jit(solution)/shard_map/all_gather | solution.py:147
  262.9 10.0 %fusion.18 = f32[1536,896]{1,0:T(8,128)S(1)} fusion(bf16[1536,2048]{1,0:T(8,128)(2,1)} %bitcast.101, bf16[1,2048,896]{2,1,0:T(8,128)(2,1)} %param.25), kind=kOutput, calls=%fused_computation.38 | convolution fusion | flops 5637144576 | bytes 15466496 | tf_op jit(solution)/shard_map/dot_general | solution.py:14
  272.9 7.1 %multiply_convert_fusion = bf16[1536,896]{1,0:T(8,128)(2,1)S(1)} fusion(f32[1536,896]{1,0:T(8,128)S(1)} %fusion.18, bf16[1536,2048]{1,0:T(8,128)(2,1)S(1)} %bitcast.102, bf16[1,2048,896]{2,1,0:T(8,128)(2,1)S(1)} %copy-done.7), kind=kOutput, calls=%fused_computation.35 | convolution fusion | flops 5645402112 | bytes 18219008 | tf_op jit(solution)/shard_map/dot_general | solution.py:15
  280.0 8.7 %convert_bitcast_fusion.1 = bf16[32,1,48,2048]{3,2,0,1:T(8,128)(2,1)} fusion(bf16[32,48,896]{2,1,0:T(8,128)(2,1)S(1)} %bitcast.103, bf16[1,896,2048]{2,1,0:T(8,128)(2,1)S(1)} %copy-done.8), kind=kOutput, calls=%fused_computation.34 | convolution fusion | flops 5640290304 | bytes 12713984 | tf_op jit(solution)/shard_map/dot_general | solution.py:17
  288.8 68.5 %reduce-scatter.2.cloned.1.call-done = bf16[4,1,48,2048]{3,2,0,1:T(8,128)(2,1)} async-done(((bf16[32,1,48,2048]{3,2,0,1:T(8,128)(2,1)}), bf16[4,1,48,2048]{3,2,0,1:T(8,128)(2,1)}) %reduce-scatter.2.cloned.1.call-update) | async-done | bytes 786448 | tf_op jit(solution)/shard_map/reduce_scatter | solution.py:157
  357.3 3.7 all-to-all-start.2
  361.5 8.6 %all-to-all-done.2 = bf16[4,1,48,2048]{3,2,1,0:T(8,128)(2,1)S(1)} async-done(((bf16[4,1,48,2048]{3,2,1,0:T(8,128)(2,1)}), bf16[4,1,48,2048]{3,2,1,0:T(8,128)(2,1)S(1)}, u32[]{:S(2)}, u32[]{:S(2)}) %all-to-all-start.2) | async-done | bytes 786464 | tf_op jit(solution)/shard_map/all_to_all | solution.py:158
  370.1 0.8 gather_fusion.1
  370.9 0.3 reshape.183
  371.2 2.1 multiply_reduce_fusion
  373.3 0.7 add_convert_fusion
  (64 shorter events, 2.3 us)
Async XLA Ops:
  6.5 89.9 %all-gather.3.cloned.1.call-start = ((), (), s32[]{:S(2)}) async-start(), calls=%async_computation.4 | async-start | bytes 9437184 | tf_op jit(solution)/shard_map/all_gather | solution.py:129
  70.6 1.7 copy-start
  79.5 2.9 copy-start.4
  81.1 7.0 %copy-start.3 = (s32[48,2]{0,1:T(2,128)S(1)}, s32[48,2]{0,1:T(2,128)}, u32[]{:S(2)}) copy-start(s32[48,2]{0,1:T(2,128)} %param.28) | copy-start | bytes 1156
  81.3 15.1 %copy-start.1 = (bf16[48,2048]{1,0:T(8,128)(2,1)S(1)}, bf16[48,2048]{1,0:T(8,128)(2,1)}, u32[]{:S(2)}) copy-start(bf16[48,2048]{1,0:T(8,128)(2,1)} %param.23) | copy-start | bytes 589828
  83.2 13.1 %all-to-all-start = ((bf16[8,48,256]{2,1,0:T(8,128)(2,1)}), bf16[8,48,256]{2,1,0:T(8,128)(2,1)S(1)}, u32[]{:S(2)}, u32[]{:S(2)}) async-start(bf16[8,48,256]{2,1,0:T(8,128)(2,1)} %multiply_convert_fusion.2), calls=%async_computation | async-start | bytes 393216 | tf_op jit(solution)/shard_map/all_to_all | solution.py:126
  88.0 174.9 %all-gather.5.cloned.1.call-start = ((), (), s32[]{:S(2)}) async-start(), calls=%async_computation.5 | async-start | bytes 7077888 | tf_op jit(solution)/shard_map/all_gather | solution.py:147
  96.4 5.1 %copy-start.2 = (f32[2048]{0:T(1024)S(1)}, f32[2048]{0:T(1024)}, u32[]{:S(2)}) copy-start(f32[2048]{0:T(1024)} %param.24) | copy-start | bytes 24580
  199.3 158.0 %reduce-scatter.2.cloned.1.call-start = ((), (), s32[]{:S(2)}) async-start(), calls=%async_computation.6 | async-start | bytes 7077888 | tf_op jit(solution)/shard_map/reduce_scatter | solution.py:157
  262.9 10.0 %copy-start.6 = (bf16[32,1,48,2048]{3,2,1,0:T(8,128)(2,1)S(1)}, bf16[32,1,48,2048]{3,2,1,0:T(8,128)(2,1)}, u32[]{:S(2)}) copy-start(bf16[32,1,48,2048]{3,2,1,0:T(8,128)(2,1)} %all-gather.5.cloned.1.call-done) | copy-start | bytes 18874372
  262.9 10.0 %copy-start.7 = (bf16[1,2048,896]{2,1,0:T(8,128)(2,1)S(1)}, bf16[1,2048,896]{2,1,0:T(8,128)(2,1)}, u32[]{:S(2)}) copy-start(bf16[1,2048,896]{2,1,0:T(8,128)(2,1)} %param.26) | copy-start | bytes 11010052
  272.9 7.1 %copy-start.8 = (bf16[1,896,2048]{2,1,0:T(8,128)(2,1)S(1)}, bf16[1,896,2048]{2,1,0:T(8,128)(2,1)}, u32[]{:S(2)}) copy-start(bf16[1,896,2048]{2,1,0:T(8,128)(2,1)} %param.27) | copy-start | bytes 11010052
  288.8 72.6 %copy-start.5 = (f32[48,2]{0,1:T(2,128)S(1)}, f32[48,2]{0,1:T(2,128)}, u32[]{:S(2)}) copy-start(f32[48,2]{0,1:T(2,128)} %param.29) | copy-start | bytes 1156
  357.3 12.7 %all-to-all-start.2 = ((bf16[4,1,48,2048]{3,2,1,0:T(8,128)(2,1)}), bf16[4,1,48,2048]{3,2,1,0:T(8,128)(2,1)S(1)}, u32[]{:S(2)}, u32[]{:S(2)}) async-start(bf16[4,1,48,2048]{3,2,1,0:T(8,128)(2,1)} %bitcast.96), calls=%async_computation.3 | async-start | bytes 1572864 | tf_op jit(solution)/shard_map/all_to_all | solution.py:158
Sparse Core Ops, SparseCore 0:
  8.9 84.8 all-gather.2
  199.4 63.4 all-gather.4
  288.9 68.3 reduce-scatter.1
where the time goes:
time: 382 us; the launch traced here: 380 us
  waiting for transfers between devices  148 us (39%)
  blocking collectives  133 us (35%)
  matrix products  35.5 us (9%)
  other arithmetic  26.7 us (7%)
  local copies, waits for them, and re-layouts  14.7 us (4%)
  between operations  13.4 us (4%)
  starting transfers between devices  8.62 us (2%)
    all_to_all x1, blocking collectives, on_device(): lax.all_to_all(outgoing.reshape(seq_devices, local_experts, capacity, mod...  96.4 us
    reduce_scatter x1, waiting for transfers between devices, on_device(): lax.psum_scatter(partials.astype(jnp.bfloat16), 'tp', scatter_dimension=0...  68.5 us
    all_gather x1, waiting for transfers between devices, on_device(): row_piece = lax.all_gather(arrived, 'tp', axis=0, tiled=True)  63.5 us
    another operation x2, other arithmetic  14.1 us
    all_gather x1, blocking collectives, on_device(): key_piece = lax.all_gather(keys, 'sp', axis=0, tiled=True)  13.4 us
    all_gather x1, blocking collectives, on_device(): value_piece = lax.all_gather(values, 'sp', axis=0, tiled=True)  12.4 us
    all_gather x1, blocking collectives, on_device(): bias_piece = lax.all_gather(key_bias, 'sp', axis=0, tiled=True)  11 us
    dot_general x1, matrix products, expert_partial(): jnp.dot(row_block, gate_matrix, preferred_element_type=jnp.float32)  9.96 us
  transfers between devices with their start and end apart: 5, of which 4 were waited for; matrix products, arithmetic and copies ran while one was open for 10% of the time, Pallas kernels for 0%

commit v1 on v0

--- a/solution.py
+++ b/solution.py
@@ -2,6 +2,7 @@
 import jax.numpy as jnp
 from jax import lax
 from jax.sharding import PartitionSpec as P
+from jax.lax import all_gather
 
 epsilon = 1e-06
 
@@ -88,8 +89,16 @@
         jnp.zeros((seq_devices, heads_here, rows_own), jnp.float32),
     )
     key_piece = lax.all_gather(keys, "sp", axis=0, tiled=True)
-    value_piece = lax.all_gather(values, "sp", axis=0, tiled=True)
-    bias_piece = lax.all_gather(key_bias, "sp", axis=0, tiled=True)
+
+    def _pair_joints(buf, field):
+        u_next = jnp.split(
+            all_gather(jnp.concatenate([field, buf], 1), "sp", axis=0, tiled=True),
+            [field.shape[1]],
+            1,
+        )
+        return u_next
+
+    value_piece, bias_piece = _pair_joints(key_bias, values)
 
     def visit(block_count, state_in):
         offset = block_count * rows_own

time: 382 us -> 373 us (0.976)
  blocking collectives: 133 us -> 115 us
  waiting for transfers between devices: 148 us -> 158 us
    all_to_all x1, blocking collectives: 96.4 us -> 86.9 us  [on_device(): lax.all_to_all(outgoing.reshape(seq_devices, local_experts, capacity, mod...]
    all_gather x2 -> x1, blocking collectives: 23.3 us -> 15.2 us  [_pair_joints(): all_gather(jnp.concatenate([field, buf], 1), 'sp', axis=0, tiled=True)]
    all_to_all x1, waiting for transfers between devices: 6.81 us -> 12.2 us  [on_device(): lax.all_to_all(attended, 'tp', split_axis=0, concat_axis=1, tiled=True)]
    all_gather x1, waiting for transfers between devices: 0.02 us -> 4.22 us  [on_device(): lax.all_gather(out_weight, 'tp', axis=0, tiled=True)]
  transfers between devices with their start and end apart: 5 -> 5, of which waited for: 4 -> 5; matrix products, arithmetic and copies ran while one was open for 10% -> 11% of each run, Pallas kernels for 0% -> 0%
where the time goes in v1:
time: 373 us; the launch traced here: 372 us
  waiting for transfers between devices  158 us (42%)
  blocking collectives  115 us (31%)
  matrix products  35.5 us (10%)
  other arithmetic  27.4 us (7%)
  local copies, waits for them, and re-layouts  14.4 us (4%)
  between operations  13.4 us (4%)
  starting transfers between devices  8.53 us (2%)
    all_to_all x1, blocking collectives, on_device(): lax.all_to_all(outgoing.reshape(seq_devices, local_experts, capacity, mod...  86.9 us
    reduce_scatter x1, waiting for transfers between devices, on_device(): lax.psum_scatter(partials.astype(jnp.bfloat16), 'tp', scatter_dimension=0...  68.5 us
    all_gather x1, waiting for transfers between devices, on_device(): row_piece = lax.all_gather(arrived, 'tp', axis=0, tiled=True)  63.5 us
    all_gather x1, blocking collectives, _pair_joints(): all_gather(jnp.concatenate([field, buf], 1), 'sp', axis=0, tiled=True)  15.2 us
    another operation x2, other arithmetic  14.1 us
    all_gather x1, blocking collectives, on_device(): key_piece = lax.all_gather(keys, 'sp', axis=0, tiled=True)  13 us
    all_to_all x1, waiting for transfers between devices, on_device(): lax.all_to_all(attended, 'tp', split_axis=0, concat_axis=1, tiled=True)  12.2 us
    dot_general x1, matrix products, expert_partial(): jnp.dot(row_block, gate_matrix, preferred_element_type=jnp.float32)  9.96 us
  transfers between devices with their start and end apart: 5, of which 5 were waited for; matrix products, arithmetic and copies ran while one was open for 11% of the time, Pallas kernels for 0%

profile of v1, /device:TPU:0, one launch (start us, length us, event | category | flops | bytes accessed | tf_op | source)
XLA Modules:
  0.0 372.5 jit_solution(1242301515541195652)
XLA Ops:
  6.5 0.7 all-gather.3.cloned.1.call-update
  7.3 1.1 copy.81
  8.4 0.7 pad_maximum_fusion
  9.1 15.2 %all_gather.12 = bf16[1536,260]{0,1:T(8,128)(2,1)S(1)} all-gather(bf16[384,260]{0,1:T(8,128)(2,1)S(1)} %pad_maximum_fusion), channel_id=1, replica_groups=mesh['sp'=4,'tp'=8] {'sp'}, dimensions={0}, use_global_device_ids=true | all-gather | bytes 998400 | tf_op jit(solution)/shard_map/all_gather | solution.py:95
  24.3 1.0 split.8
  25.3 0.6 split.9
  26.0 0.8 copy.83
  26.9 13.0 %all_gather.13 = bf16[1536,256]{0,1:T(8,128)(2,1)} all-gather(bf16[384,256]{0,1:T(8,128)(2,1)S(1)} %copy.82), channel_id=1, replica_groups=mesh['sp'=4,'tp'=8] {'sp'}, dimensions={0}, use_global_device_ids=true | all-gather | bytes 983040 | tf_op jit(solution)/shard_map/all_gather | solution.py:91
  39.9 1.3 broadcast_in_dim.84
  41.2 0.6 broadcast_in_dim.85
  41.8 28.1 %while.17 = (s32[]{:T(128)}, f32[4,384,256]{1,2,0:T(8,128)}, f32[4,4,384]{2,1,0:T(4,128)}, s32[]{:T(128)}, bf16[1536,256]{0,1:T(8,128)(2,1)}, /*index=5*/bf16[15...) while((s32[]{:T(128)}, f32[4,384,256]{1,2,0:T(8,128)}, ...), condition=%wide.region_6.7_spmd.clone.clone, body=%wide.region_0.6_spmd.clone.clone.sunk | while | flops 246117120 | bytes 38572464 | solution.py:123
  41.8 27.9 %conditional.4 = ((f32[4,384,256]{1,2,0:T(8,128)}, f32[4,4,384]{2,1,0:T(4,128)})) conditional(s32[]{:T(128)} %convert_element_type.76, (f32[4,384,256]{1,2,0:T(8,128)}, f32[4,4,384]{2,1,0:T(4,128)}) %tuple.53, (s32[]{:T(128)}, bf16[1536,256]{0,1:T(8,128)(2,1)}, s32[]{:T(128)}, bf16[1536,256]{0,1:T(8,128)(2,1)}, bf16[384,4,64]{0,2,1:T(8,128)(2,1)}, ...), branch_computations={%region_1.0_spmd, %region_2.5_spmd} | conditional | flops 246117120 | bytes 38570716 | solution.py:121
  41.8 1.1 constant_dynamic-slice_fusion
  42.8 0.7 convert_bitcast_fusion
  43.7 4.3 %fusion.15 = (f32[4,384]{1,0:T(4,128)S(1)}, f32[4,384,384]{1,2,0:T(8,128)S(1)}, f32[4,384,384]{2,1,0:T(8,128)}) fusion(f32[4,384]{1,0:T(4,128)S(1)} %convert_bitcast_fusion, pred[384,384]{0,1:T(8,128)(4,1)S(1)} %broadcast_compare_fusion, bf16[384,4,64]{0,2,1:T(8,128)(2,1)S(1)} %bitcast.92, bf16[384,4,64]{0,2,1:T(8,128)(2,1)} %get-tuple-element.177), kind=kOutput, calls=%fused_computation.33 | convolution fusion | flops 81984000 | bytes 5271552 | tf_op jit(solution)/shard_map/while/body/eval_jaxpr/cond/branch_1_fun/qhd,khd->hqk/dot_general | solution.py:64
  48.0 14.0 %fusion.2 = f32[4,384,3,128]{1,2,3,0:T(4,128)S(1)} fusion(f32[4,384,3,128]{1,3,2,0:T(8,128)S(1)} %bitcast.88), kind=kOutput, calls=%fused_computation.5 | output fusion | flops 74907648 | bytes 4718592 | tf_op jit(solution)/shard_map/reduce-window
  62.1 0.5 broadcast_add_fusion
  62.6 0.2 copy.79
  62.9 1.4 copy-done
  64.3 3.6 fusion.8
  67.9 0.3 fusion.27
  68.3 0.8 constant_dynamic-update-slice_fusion
  69.1 0.6 bitcast_dynamic-update-slice_fusion
  69.9 0.8 reduce_sum.74
  70.7 0.8 fusion.24
  71.4 1.6 fusion.22
  73.1 0.2 copy.84
  73.5 0.5 mul.104
  73.9 0.5 mul.105
  74.5 0.7 multiply_convert_fusion.2
  75.2 4.7 %all-to-all-start = ((bf16[8,48,256]{2,1,0:T(8,128)(2,1)}), bf16[8,48,256]{2,1,0:T(8,128)(2,1)S(1)}, u32[]{:S(2)}, u32[]{:S(2)}) async-start(bf16[8,48,256]{2,1,0:T(8,128)(2,1)} %multiply_convert_fusion.2), calls=%async_computation | async-start | bytes 393216 | tf_op jit(solution)/shard_map/all_to_all | solution.py:135
  80.5 0.2 select_reduce_fusion.1
  81.5 12.2 %all-to-all-done = bf16[8,48,256]{2,1,0:T(8,128)(2,1)S(1)} async-done(((bf16[8,48,256]{2,1,0:T(8,128)(2,1)}), bf16[8,48,256]{2,1,0:T(8,128)(2,1)S(1)}, u32[]{:S(2)}, u32[]{:S(2)}) %all-to-all-start) | async-done | bytes 196640 | tf_op jit(solution)/shard_map/all_to_all | solution.py:135
  93.7 4.2 %all-gather.3.cloned.1.call-done = bf16[2048,2048]{1,0:T(8,128)(2,1)} async-done(((bf16[256,2048]{1,0:T(8,128)(2,1)}), bf16[2048,2048]{1,0:T(8,128)(2,1)}) %all-gather.3.cloned.1.call-update) | async-done | bytes 8388624 | tf_op jit(solution)/shard_map/all_gather | solution.py:138
  97.9 5.1 %multiply_reduce_fusion.1 = (f32[48]{0:T(128)S(1)}, f32[48,2048]{1,0:T(8,128)S(1)}) fusion(bf16[48,2048]{1,0:T(8,128)(2,1)S(1)} %bitcast.94, bf16[2048,2048]{1,0:T(8,128)(2,1)} %all-gather.3.cloned.1.call-done, bf16[48,2048]{1,0:T(8,128)(2,1)S(1)} %copy-done.1), kind=kOutput, calls=%fused_computation.54 | convolution fusion | flops 403242944 | bytes 9175232 | tf_op jit(solution)/shard_map/dot_general | solution.py:136
  103.1 1.1 gather_fusion
  104.4 86.9 %all_to_all.26 = bf16[4,1,48,2048]{3,2,1,0:T(8,128)(2,1)} all-to-all(bf16[4,1,48,2048]{3,2,1,0:T(8,128)(2,1)S(1)} %broadcast_select_fusion), channel_id=1, replica_groups=mesh['sp'=4,'tp'=8] {'sp'}, dimensions={0} | all-to-all | bytes 1572864 | tf_op jit(solution)/shard_map/all_to_all | solution.py:149
  191.4 63.5 %all-gather.5.cloned.1.call-done = bf16[32,1,48,2048]{3,2,1,0:T(8,128)(2,1)} async-done(((bf16[4,1,48,2048]{3,2,1,0:T(8,128)(2,1)}), bf16[32,1,48,2048]{3,2,1,0:T(8,128)(2,1)}) %all-gather.5.cloned.1.call-update) | async-done | bytes 6291472 | tf_op jit(solution)/shard_map/all_gather | solution.py:156
  254.9 10.0 %fusion.18 = f32[1536,896]{1,0:T(8,128)S(1)} fusion(bf16[1536,2048]{1,0:T(8,128)(2,1)} %bitcast.101, bf16[1,2048,896]{2,1,0:T(8,128)(2,1)} %param.25), kind=kOutput, calls=%fused_computation.38 | convolution fusion | flops 5637144576 | bytes 15466496 | tf_op jit(solution)/shard_map/dot_general | solution.py:15
  264.9 7.1 %multiply_convert_fusion = bf16[1536,896]{1,0:T(8,128)(2,1)S(1)} fusion(f32[1536,896]{1,0:T(8,128)S(1)} %fusion.18, bf16[1536,2048]{1,0:T(8,128)(2,1)S(1)} %bitcast.102, bf16[1,2048,896]{2,1,0:T(8,128)(2,1)S(1)} %copy-done.9), kind=kOutput, calls=%fused_computation.35 | convolution fusion | flops 5645402112 | bytes 18219008 | tf_op jit(solution)/shard_map/dot_general | solution.py:16
  272.0 8.7 %convert_bitcast_fusion.1 = bf16[32,1,48,2048]{3,2,0,1:T(8,128)(2,1)} fusion(bf16[32,48,896]{2,1,0:T(8,128)(2,1)S(1)} %bitcast.103, bf16[1,896,2048]{2,1,0:T(8,128)(2,1)S(1)} %copy-done.10), kind=kOutput, calls=%fused_computation.34 | convolution fusion | flops 5640290304 | bytes 12713984 | tf_op jit(solution)/shard_map/dot_general | solution.py:18
  280.8 68.5 %reduce-scatter.2.cloned.1.call-done = bf16[4,1,48,2048]{3,2,0,1:T(8,128)(2,1)} async-done(((bf16[32,1,48,2048]{3,2,0,1:T(8,128)(2,1)}), bf16[4,1,48,2048]{3,2,0,1:T(8,128)(2,1)}) %reduce-scatter.2.cloned.1.call-update) | async-done | bytes 786448 | tf_op jit(solution)/shard_map/reduce_scatter | solution.py:166
  349.3 3.7 all-to-all-start.2
  353.5 8.6 %all-to-all-done.2 = bf16[4,1,48,2048]{3,2,1,0:T(8,128)(2,1)S(1)} async-done(((bf16[4,1,48,2048]{3,2,1,0:T(8,128)(2,1)}), bf16[4,1,48,2048]{3,2,1,0:T(8,128)(2,1)S(1)}, u32[]{:S(2)}, u32[]{:S(2)}) %all-to-all-start.2) | async-done | bytes 786464 | tf_op jit(solution)/shard_map/all_to_all | solution.py:167
  362.1 0.8 gather_fusion.1
  362.9 0.3 reshape.183
  363.2 2.1 multiply_reduce_fusion
  365.2 0.7 add_convert_fusion
  (70 shorter events, 2.7 us)
Async XLA Ops:
  6.5 19.3 %copy-start.2 = (bf16[384,256]{1,0:T(8,128)(2,1)S(1)}, bf16[384,256]{1,0:T(8,128)(2,1)}, u32[]{:S(2)}) copy-start(bf16[384,256]{1,0:T(8,128)(2,1)} %param.18) | copy-start | bytes 589828
  6.5 19.5 %copy-start.3 = (bf16[384,256]{1,0:T(8,128)(2,1)S(1)}, bf16[384,256]{1,0:T(8,128)(2,1)}, u32[]{:S(2)}) copy-start(bf16[384,256]{1,0:T(8,128)(2,1)} %param.17) | copy-start | bytes 589828
  6.5 91.4 %all-gather.3.cloned.1.call-start = ((), (), s32[]{:S(2)}) async-start(), calls=%async_computation.4 | async-start | bytes 9437184 | tf_op jit(solution)/shard_map/all_gather | solution.py:138
  62.6 1.7 copy-start
  71.4 3.0 copy-start.6
  73.1 7.0 %copy-start.5 = (s32[48,2]{0,1:T(2,128)S(1)}, s32[48,2]{0,1:T(2,128)}, u32[]{:S(2)}) copy-start(s32[48,2]{0,1:T(2,128)} %param.28) | copy-start | bytes 1156
  73.3 24.6 %copy-start.1 = (bf16[48,2048]{1,0:T(8,128)(2,1)S(1)}, bf16[48,2048]{1,0:T(8,128)(2,1)}, u32[]{:S(2)}) copy-start(bf16[48,2048]{1,0:T(8,128)(2,1)} %param.23) | copy-start | bytes 589828
  75.2 18.4 %all-to-all-start = ((bf16[8,48,256]{2,1,0:T(8,128)(2,1)}), bf16[8,48,256]{2,1,0:T(8,128)(2,1)S(1)}, u32[]{:S(2)}, u32[]{:S(2)}) async-start(bf16[8,48,256]{2,1,0:T(8,128)(2,1)} %multiply_convert_fusion.2), calls=%async_computation | async-start | bytes 393216 | tf_op jit(solution)/shard_map/all_to_all | solution.py:135
  80.0 174.9 %all-gather.5.cloned.1.call-start = ((), (), s32[]{:S(2)}) async-start(), calls=%async_computation.5 | async-start | bytes 7077888 | tf_op jit(solution)/shard_map/all_gather | solution.py:156
  97.9 5.1 %copy-start.4 = (f32[2048]{0:T(1024)S(1)}, f32[2048]{0:T(1024)}, u32[]{:S(2)}) copy-start(f32[2048]{0:T(1024)} %param.24) | copy-start | bytes 24580
  191.3 158.0 %reduce-scatter.2.cloned.1.call-start = ((), (), s32[]{:S(2)}) async-start(), calls=%async_computation.6 | async-start | bytes 7077888 | tf_op jit(solution)/shard_map/reduce_scatter | solution.py:166
  254.9 10.0 %copy-start.8 = (bf16[32,1,48,2048]{3,2,1,0:T(8,128)(2,1)S(1)}, bf16[32,1,48,2048]{3,2,1,0:T(8,128)(2,1)}, u32[]{:S(2)}) copy-start(bf16[32,1,48,2048]{3,2,1,0:T(8,128)(2,1)} %all-gather.5.cloned.1.call-done) | copy-start | bytes 18874372
  254.9 10.0 %copy-start.9 = (bf16[1,2048,896]{2,1,0:T(8,128)(2,1)S(1)}, bf16[1,2048,896]{2,1,0:T(8,128)(2,1)}, u32[]{:S(2)}) copy-start(bf16[1,2048,896]{2,1,0:T(8,128)(2,1)} %param.26) | copy-start | bytes 11010052
  264.9 7.1 %copy-start.10 = (bf16[1,896,2048]{2,1,0:T(8,128)(2,1)S(1)}, bf16[1,896,2048]{2,1,0:T(8,128)(2,1)}, u32[]{:S(2)}) copy-start(bf16[1,896,2048]{2,1,0:T(8,128)(2,1)} %param.27) | copy-start | bytes 11010052
  280.8 72.6 %copy-start.7 = (f32[48,2]{0,1:T(2,128)S(1)}, f32[48,2]{0,1:T(2,128)}, u32[]{:S(2)}) copy-start(f32[48,2]{0,1:T(2,128)} %param.29) | copy-start | bytes 1156
  349.3 12.8 %all-to-all-start.2 = ((bf16[4,1,48,2048]{3,2,1,0:T(8,128)(2,1)}), bf16[4,1,48,2048]{3,2,1,0:T(8,128)(2,1)S(1)}, u32[]{:S(2)}, u32[]{:S(2)}) async-start(bf16[4,1,48,2048]{3,2,1,0:T(8,128)(2,1)} %bitcast.96), calls=%async_computation.3 | async-start | bytes 1572864 | tf_op jit(solution)/shard_map/all_to_all | solution.py:167
Sparse Core Ops, SparseCore 0:
  8.9 88.9 all-gather.2
  191.4 63.4 all-gather.4
  280.9 68.3 reduce-scatter.1
